TPU v7x, 32 devices: a whole 2x2x4 slice. The times are simulated.
32 devices in a mesh: kv: 8 (over z, y), tp: 4 (over x, core).
Axes of the slice: x: 2, y: 2, z: 4, core: 2. Of those that a mesh axis runs over, the one named last changes fastest.
Arguments:
- queries: bfloat16 [2048, 3072], P('kv', 'tp'), may hold values from -6 to 6
- key_vectors: bfloat16 [2048, 512], P('kv', 'tp'), may hold values from -6 to 6
- value_vectors: bfloat16 [2048, 512], P('kv', 'tp'), may hold values from -6 to 6
- log_sums: float32 [2048, 48], P('kv', 'tp'), may hold values from 4.5 to 6.5
- out_grad: bfloat16 [2048, 3072], P('kv', 'tp'), may hold values from -48 to 48
- layer_input: bfloat16 [2048, 3072], P('kv', 'tp'), may hold values from -0.29882812 to 0.29882812
- chosen: int32 [32, 16], P('kv'), may hold values from -1 to 55, as said below
Outputs:
- query_grad: bfloat16 [2048, 3072], P('kv', 'tp')
- key_grad: bfloat16 [2048, 512], P('kv', 'tp')
- value_grad: bfloat16 [2048, 512], P('kv', 'tp')
- weight_grad: float32 [3072, 512], P('kv', 'tp')
Inputs may be any that keep to these rules, and one draw needn't show every extreme that they name: `chosen`: each entry is -1 or the number c of a block of 32 positions (c * 32 to c * 32 + 31) that lies wholly within an earlier index of kv than its query block. The numbers of one row differ, and all query blocks held by one index of kv together take at most one block from each other index.
All inputs are finite; a program needn't handle non-finite values.
Results may differ from a plain program's by a relative error of at most 0.0061.
Values may be sent and summed in bfloat16 or wider, within the bound.
No kernel may reach another device: no remote copies, remote signals or barrier semaphores. Data moves between devices by JAX's collectives and lax.ppermute only.
A program may use at most 64 MiB of HBM per device.

v0:
```python
import jax
import jax.numpy as jnp
from jax import lax
from jax.sharding import PartitionSpec as P

HEAD = 64
KB = 32
QB = 64
NSEL = 16


def per_device(queries, key_vectors, value_vectors, log_sums, out_grad, layer_input, chosen):
    axis_count = lax.axis_size("kv")
    own_index = lax.axis_index("kv")
    span_rows = queries.shape[0]
    kv_local = key_vectors.shape[1] // HEAD
    group_size = queries.shape[1] // key_vectors.shape[1]
    blocks_here = span_rows // KB
    query_blocks = span_rows // QB
    score_scale = HEAD ** (-0.5)
    half_width = kv_local * HEAD
    pair_width = 2 * half_width
    paired = jnp.concatenate([key_vectors, value_vectors], axis=1)
    owners = jnp.arange(axis_count, dtype=jnp.int32)
    usable = chosen >= 0
    owner_of = jnp.where(usable, chosen // blocks_here, -1)
    within = chosen - chosen // blocks_here * blocks_here
    matched = owner_of[:, :, None] == owners[None, None, :]
    wanted = jnp.max(jnp.where(matched, within[:, :, None], -1), axis=(0, 1))
    incoming = lax.all_to_all(wanted[:, None], "kv", split_axis=0, concat_axis=0, tiled=True)[:, 0]
    blocks = paired.reshape(blocks_here, KB, pair_width)
    outgoing = jnp.where(
        (incoming >= 0)[:, None, None],
        blocks[jnp.maximum(incoming, 0)],
        jnp.zeros((), paired.dtype),
    )
    fetched = lax.all_to_all(outgoing, "kv", split_axis=0, concat_axis=0, tiled=True)
    query_parts = queries.reshape(query_blocks, QB, kv_local, group_size, HEAD)
    grad_parts = out_grad.reshape(query_blocks, QB, kv_local, group_size, HEAD)
    sum_parts = log_sums.reshape(query_blocks, QB, kv_local, group_size)
    slot_owner = jnp.clip(owner_of, 0, axis_count - 1)
    key_own = key_vectors.reshape(span_rows, kv_local, HEAD)
    value_own = value_vectors.reshape(span_rows, kv_local, HEAD)
    key_pos = own_index * span_rows + jnp.arange(span_rows, dtype=jnp.int32)

    def one_block(packed):
        query_part, grad_part, sum_part, slot_part, usable_part, block_index = packed
        selected = fetched[slot_part].reshape(NSEL * KB, 2, kv_local, HEAD)
        key_sel = selected[:, 0]
        value_sel = selected[:, 1]
        keep_key = jnp.repeat(usable_part, KB)
        query_pos = own_index * span_rows + block_index * QB + jnp.arange(QB, dtype=jnp.int32)
        causal = key_pos[None, :] <= query_pos[:, None]
        score_sel = (
            jnp.einsum("qhgd,khd->qhgk", query_part, key_sel, preferred_element_type=jnp.float32)
            * score_scale
        )
        score_own = (
            jnp.einsum("qhgd,khd->qhgk", query_part, key_own, preferred_element_type=jnp.float32)
            * score_scale
        )
        weight_sel = jnp.where(
            keep_key[None, None, None, :], jnp.exp(score_sel - sum_part[..., None]), 0.0
        )
        weight_own = jnp.where(
            causal[:, None, None, :], jnp.exp(score_own - sum_part[..., None]), 0.0
        )
        round_sel = weight_sel.astype(jnp.bfloat16)
        round_own = weight_own.astype(jnp.bfloat16)
        output = jnp.einsum(
            "qhgk,khd->qhgd", round_sel, value_sel, preferred_element_type=jnp.float32
        )
        output = output + jnp.einsum(
            "qhgk,khd->qhgd", round_own, value_own, preferred_element_type=jnp.float32
        )
        row_delta = jnp.sum(grad_part.astype(jnp.float32) * output, axis=-1)
        prod_sel = jnp.einsum(
            "qhgd,khd->qhgk", grad_part, value_sel, preferred_element_type=jnp.float32
        )
        prod_own = jnp.einsum(
            "qhgd,khd->qhgk", grad_part, value_own, preferred_element_type=jnp.float32
        )
        slope_sel = (weight_sel * (prod_sel - row_delta[..., None])).astype(jnp.bfloat16)
        slope_own = (weight_own * (prod_own - row_delta[..., None])).astype(jnp.bfloat16)
        query_total = jnp.einsum(
            "qhgk,khd->qhgd", slope_sel, key_sel, preferred_element_type=jnp.float32
        )
        query_total = query_total + jnp.einsum(
            "qhgk,khd->qhgd", slope_own, key_own, preferred_element_type=jnp.float32
        )
        query_out = (query_total * score_scale).astype(jnp.bfloat16)
        key_sel_grad = (
            jnp.einsum("qhgk,qhgd->khd", slope_sel, query_part, preferred_element_type=jnp.float32)
            * score_scale
        )
        value_sel_grad = jnp.einsum(
            "qhgk,qhgd->khd", round_sel, grad_part, preferred_element_type=jnp.float32
        )
        key_own_grad = (
            jnp.einsum("qhgk,qhgd->khd", slope_own, query_part, preferred_element_type=jnp.float32)
            * score_scale
        )
        value_own_grad = jnp.einsum(
            "qhgk,qhgd->khd", round_own, grad_part, preferred_element_type=jnp.float32
        )
        sel_pair = jnp.concatenate(
            [
                key_sel_grad.reshape(NSEL, KB, half_width),
                value_sel_grad.reshape(NSEL, KB, half_width),
            ],
            axis=2,
        )
        own_pair = jnp.concatenate(
            [
                key_own_grad.reshape(span_rows, half_width),
                value_own_grad.reshape(span_rows, half_width),
            ],
            axis=1,
        )
        return (query_out, sel_pair, own_pair)

    block_ids = jnp.arange(query_blocks, dtype=jnp.int32)
    query_outs, sel_pairs, own_pairs = lax.map(
        one_block, (query_parts, grad_parts, sum_parts, slot_owner, usable, block_ids)
    )
    onehot = ((slot_owner[:, :, None] == owners[None, None, :]) & usable[:, :, None]).astype(
        jnp.float32
    )
    onehot = onehot.reshape(query_blocks * NSEL, axis_count)
    per_owner = jnp.einsum(
        "so,sr->or",
        onehot,
        sel_pairs.reshape(query_blocks * NSEL, KB * pair_width),
        precision=lax.Precision.HIGHEST,
    )
    returned = lax.all_to_all(
        per_owner.reshape(axis_count, KB, pair_width), "kv", split_axis=0, concat_axis=0, tiled=True
    )
    placing = (incoming[None, :] == jnp.arange(blocks_here, dtype=jnp.int32)[:, None]).astype(
        jnp.float32
    )
    landed = jnp.einsum(
        "bs,sr->br",
        placing,
        returned.reshape(axis_count, KB * pair_width),
        precision=lax.Precision.HIGHEST,
    )
    totals = jnp.sum(own_pairs, axis=0) + landed.reshape(span_rows, pair_width)
    key_grad = totals[:, :half_width].astype(jnp.bfloat16)
    value_grad = totals[:, half_width:].astype(jnp.bfloat16)
    full_input = lax.all_gather(layer_input, "tp", axis=1, tiled=True)
    weight_grad = lax.psum_scatter(
        lax.dot_general(
            full_input, key_grad, (((0,), (0,)), ((), ())), preferred_element_type=jnp.float32
        ),
        "kv",
        scatter_dimension=0,
        tiled=True,
    )
    return (query_outs.reshape(span_rows, queries.shape[1]), key_grad, value_grad, weight_grad)


def solution(mesh):
    placed = (
        P("kv", "tp"),
        P("kv", "tp"),
        P("kv", "tp"),
        P("kv", "tp"),
        P("kv", "tp"),
        P("kv", "tp"),
        P("kv", None),
    )
    return jax.shard_map(
        per_device,
        mesh=mesh,
        in_specs=placed,
        out_specs=(P("kv", "tp"), P("kv", "tp"), P("kv", "tp"), P("kv", "tp")),
        check_vma=False,
    )
```

profile of v0, /device:TPU:0, one launch (start us, length us, event | category | flops | bytes accessed | tf_op | source)
XLA Modules:
  0.0 224.7 jit_solution(12152546866315410712)
XLA Ops:
  9.3 7.3 %all-to-all-start = ((s32[8,1,1]{2,1,0:T(1,128)}), s32[8,1,1]{2,1,0:T(1,128)S(1)}, u32[]{:S(2)}, u32[]{:S(2)}) async-start(s32[8,1,1]{2,1,0:T(1,128)} %copy.110), calls=%async_computation | async-start | bytes 8192 | tf_op jit(solution)/shard_map/all_to_all | solution.py:30
  17.5 5.5 %all-to-all-done = s32[8,1,1]{2,1,0:T(1,128)S(1)} async-done(((s32[8,1,1]{2,1,0:T(1,128)}), s32[8,1,1]{2,1,0:T(1,128)S(1)}, u32[]{:S(2)}, u32[]{:S(2)}) %all-to-all-start) | async-done | bytes 64 | tf_op jit(solution)/shard_map/all_to_all | solution.py:30
  24.9 3.4 %all-to-all-start.1 = ((bf16[8,32,256]{2,1,0:T(8,128)(2,1)}), bf16[8,32,256]{2,1,0:T(8,128)(2,1)S(1)}, u32[]{:S(2)}, u32[]{:S(2)}) async-start(bf16[8,32,256]{2,1,0:T(8,128)(2,1)} %broadcast_select_fusion), calls=%async_computation.1 | async-start | bytes 262144 | tf_op jit(solution)/shard_map/all_to_all | solution.py:37
  29.1 1.6 copy.113
  36.9 93.2 %while.18 = (s32[]{:T(128)}, bf16[4,64,2,6,64]{1,4,3,2,0:T(8,128)(2,1)}, f32[4,16,32,256]{3,2,1,0:T(8,128)}, f32[4,256,256]{1,2,0:T(8,128)}, s32[4,16]{1,0:T(4,1...) while((s32[]{:T(128)}, ...), condition=%wide.region_3.4_spmd.clone.clone, body=%wide.region_1.3_spmd.clone.clone.sunk | while | flops 458359424 | bytes 25241412 | solution.py:123
  39.2 1.4 fusion.153
  48.6 2.0 reshape.226
  58.5 1.8 fusion.158
  62.5 1.4 fusion.153
  71.9 2.0 reshape.226
  81.7 1.8 fusion.158
  85.8 1.4 fusion.153
  95.1 2.0 reshape.226
  105.0 1.8 fusion.158
  109.1 1.4 fusion.153
  118.4 2.0 reshape.226
  128.3 1.8 fusion.158
  130.1 3.5 %fusion.66 = f32[8,32,256]{2,0,1:T(8,128)S(1)} fusion(s32[64]{0:T(128)} %eq.51, pred[64]{0:T(512)(128)(4,1)} %and.19, f32[8,8,32,256]{3,2,1,0:T(8,128)} %bitcast.274), kind=kOutput, calls=%fused_computation.90 | convolution fusion | flops 50332672 | bytes 2359616 | tf_op jit(solution)/shard_map/so,sr->or/dot_general | solution.py:130
  134.5 5.9 %all-to-all-start.2 = ((f32[8,32,256]{2,1,0:T(8,128)}), f32[8,32,256]{2,1,0:T(8,128)S(1)}, u32[]{:S(2)}, u32[]{:S(2)}) async-start(f32[8,32,256]{2,1,0:T(8,128)} %copy.120), calls=%async_computation.2 | async-start | bytes 524288 | tf_op jit(solution)/shard_map/all_to_all | solution.py:136
  140.7 7.9 %all-to-all-done.2 = f32[8,32,256]{2,1,0:T(8,128)S(1)} async-done(((f32[8,32,256]{2,1,0:T(8,128)}), f32[8,32,256]{2,1,0:T(8,128)S(1)}, u32[]{:S(2)}, u32[]{:S(2)}) %all-to-all-start.2) | async-done | bytes 262176 | tf_op jit(solution)/shard_map/all_to_all | solution.py:136
  149.3 2.9 %convolution_bitcast_fusion.8 = f32[3072,128]{0,1:T(8,128)} fusion(bf16[256,3072]{1,0:T(8,128)(2,1)} %all-gather.2.cloned.1.call-done, bf16[256,256]{0,1:T(8,128)(2,1)S(1)} %add_convert_fusion), kind=kOutput, calls=%fused_computation.89 | convolution fusion | flops 201326592 | bytes 3211264 | tf_op jit(solution)/shard_map/dot_general | solution.py:153
  154.3 1.4 reshape.213
  157.2 58.9 %reduce-scatter.2.cloned.1.call-done = f32[384,128]{0,1:T(8,128)} async-done(((f32[3072,128]{0,1:T(8,128)}), f32[384,128]{0,1:T(8,128)}) %reduce-scatter.2.cloned.1.call-update) | async-done | bytes 196624 | tf_op jit(solution)/shard_map/reduce_scatter | solution.py:152
  216.1 1.7 copy.125
  (230 shorter events, 85.8 us)
Async XLA Ops:
  7.2 23.5 %copy-start.7 = (bf16[256,128]{1,0:T(8,128)(2,1)S(1)}, bf16[256,128]{1,0:T(8,128)(2,1)}, u32[]{:S(2)}) copy-start(bf16[256,128]{1,0:T(8,128)(2,1)} %param.11) | copy-start | bytes 196612
  7.2 24.2 %copy-start.5 = (bf16[256,768]{1,0:T(8,128)(2,1)S(1)}, bf16[256,768]{1,0:T(8,128)(2,1)}, u32[]{:S(2)}) copy-start(bf16[256,768]{1,0:T(8,128)(2,1)} %param.9) | copy-start | bytes 1179652
  9.3 13.7 %all-to-all-start = ((s32[8,1,1]{2,1,0:T(1,128)}), s32[8,1,1]{2,1,0:T(1,128)S(1)}, u32[]{:S(2)}, u32[]{:S(2)}) async-start(s32[8,1,1]{2,1,0:T(1,128)} %copy.110), calls=%async_computation | async-start | bytes 8192 | tf_op jit(solution)/shard_map/all_to_all | solution.py:30
  24.9 12.0 %all-to-all-start.1 = ((bf16[8,32,256]{2,1,0:T(8,128)(2,1)}), bf16[8,32,256]{2,1,0:T(8,128)(2,1)S(1)}, u32[]{:S(2)}, u32[]{:S(2)}) async-start(bf16[8,32,256]{2,1,0:T(8,128)(2,1)} %broadcast_select_fusion), calls=%async_computation.1 | async-start | bytes 262144 | tf_op jit(solution)/shard_map/all_to_all | solution.py:37
  28.3 120.9 %all-gather.2.cloned.1.call-start = ((), (), s32[]{:S(2)}) async-start(), calls=%async_computation.4 | async-start | bytes 1966080 | tf_op jit(solution)/shard_map/all_gather | solution.py:151
  36.9 4.2 %copy-start.11 = (s32[4]{0:T(128)}, s32[4]{0:T(128)S(1)}, u32[]{:S(2)}) copy-start(s32[4]{0:T(128)S(1)} %get-tuple-element.490) | copy-start | bytes 52 | tf_op jit(solution)/shard_map/while
  53.6 4.3 %copy-start.2 = (bf16[512,1,2,64]{0,3,2,1:T(8,128)(2,1)S(1)}, bf16[512,1,2,64]{0,3,2,1:T(8,128)(2,1)}, u32[]{:S(2)}) copy-start(bf16[512,1,2,64]{0,3,2,1:T(8,128)(2,1)} %copy-done.1) | copy-start | bytes 393220 | tf_op jit(solution)/shard_map/while
  57.2 3.1 %copy-start.9 = (f32[4,64,2,6]{1,0,3,2:T(4,128)S(1)}, f32[4,64,2,6]{1,0,3,2:T(4,128)}, u32[]{:S(2)}) copy-start(f32[4,64,2,6]{1,0,3,2:T(4,128)} %copy-done.8) | copy-start | bytes 36868 | tf_op jit(solution)/shard_map/while
  57.2 3.1 %copy-start.12 = (s32[4]{0:T(128)S(1)}, s32[4]{0:T(128)}, u32[]{:S(2)}) copy-start(s32[4]{0:T(128)} %copy-done.11) | copy-start | bytes 52 | tf_op jit(solution)/shard_map/while
  60.3 4.1 %copy-start.11 = (s32[4]{0:T(128)}, s32[4]{0:T(128)S(1)}, u32[]{:S(2)}) copy-start(s32[4]{0:T(128)S(1)} %get-tuple-element.490) | copy-start | bytes 52 | tf_op jit(solution)/shard_map/while
  76.9 4.3 %copy-start.2 = (bf16[512,1,2,64]{0,3,2,1:T(8,128)(2,1)S(1)}, bf16[512,1,2,64]{0,3,2,1:T(8,128)(2,1)}, u32[]{:S(2)}) copy-start(bf16[512,1,2,64]{0,3,2,1:T(8,128)(2,1)} %copy-done.1) | copy-start | bytes 393220 | tf_op jit(solution)/shard_map/while
  80.5 3.1 %copy-start.9 = (f32[4,64,2,6]{1,0,3,2:T(4,128)S(1)}, f32[4,64,2,6]{1,0,3,2:T(4,128)}, u32[]{:S(2)}) copy-start(f32[4,64,2,6]{1,0,3,2:T(4,128)} %copy-done.8) | copy-start | bytes 36868 | tf_op jit(solution)/shard_map/while
  80.5 3.1 %copy-start.12 = (s32[4]{0:T(128)S(1)}, s32[4]{0:T(128)}, u32[]{:S(2)}) copy-start(s32[4]{0:T(128)} %copy-done.11) | copy-start | bytes 52 | tf_op jit(solution)/shard_map/while
  83.5 4.1 %copy-start.11 = (s32[4]{0:T(128)}, s32[4]{0:T(128)S(1)}, u32[]{:S(2)}) copy-start(s32[4]{0:T(128)S(1)} %get-tuple-element.490) | copy-start | bytes 52 | tf_op jit(solution)/shard_map/while
  100.2 4.3 %copy-start.2 = (bf16[512,1,2,64]{0,3,2,1:T(8,128)(2,1)S(1)}, bf16[512,1,2,64]{0,3,2,1:T(8,128)(2,1)}, u32[]{:S(2)}) copy-start(bf16[512,1,2,64]{0,3,2,1:T(8,128)(2,1)} %copy-done.1) | copy-start | bytes 393220 | tf_op jit(solution)/shard_map/while
  103.8 3.1 %copy-start.9 = (f32[4,64,2,6]{1,0,3,2:T(4,128)S(1)}, f32[4,64,2,6]{1,0,3,2:T(4,128)}, u32[]{:S(2)}) copy-start(f32[4,64,2,6]{1,0,3,2:T(4,128)} %copy-done.8) | copy-start | bytes 36868 | tf_op jit(solution)/shard_map/while
  103.8 3.1 %copy-start.12 = (s32[4]{0:T(128)S(1)}, s32[4]{0:T(128)}, u32[]{:S(2)}) copy-start(s32[4]{0:T(128)} %copy-done.11) | copy-start | bytes 52 | tf_op jit(solution)/shard_map/while
  106.9 4.1 %copy-start.11 = (s32[4]{0:T(128)}, s32[4]{0:T(128)S(1)}, u32[]{:S(2)}) copy-start(s32[4]{0:T(128)S(1)} %get-tuple-element.490) | copy-start | bytes 52 | tf_op jit(solution)/shard_map/while
  123.5 4.3 %copy-start.2 = (bf16[512,1,2,64]{0,3,2,1:T(8,128)(2,1)S(1)}, bf16[512,1,2,64]{0,3,2,1:T(8,128)(2,1)}, u32[]{:S(2)}) copy-start(bf16[512,1,2,64]{0,3,2,1:T(8,128)(2,1)} %copy-done.1) | copy-start | bytes 393220 | tf_op jit(solution)/shard_map/while
  127.0 3.1 %copy-start.9 = (f32[4,64,2,6]{1,0,3,2:T(4,128)S(1)}, f32[4,64,2,6]{1,0,3,2:T(4,128)}, u32[]{:S(2)}) copy-start(f32[4,64,2,6]{1,0,3,2:T(4,128)} %copy-done.8) | copy-start | bytes 36868 | tf_op jit(solution)/shard_map/while
  127.0 3.1 %copy-start.12 = (s32[4]{0:T(128)S(1)}, s32[4]{0:T(128)}, u32[]{:S(2)}) copy-start(s32[4]{0:T(128)} %copy-done.11) | copy-start | bytes 52 | tf_op jit(solution)/shard_map/while
  130.1 10.5 %copy-start.3 = (f32[4,256,256]{1,2,0:T(8,128)S(1)}, f32[4,256,256]{1,2,0:T(8,128)}, u32[]{:S(2)}) copy-start(f32[4,256,256]{1,2,0:T(8,128)} %get-tuple-element.178) | copy-start | bytes 3145732
  134.5 14.1 %all-to-all-start.2 = ((f32[8,32,256]{2,1,0:T(8,128)}), f32[8,32,256]{2,1,0:T(8,128)S(1)}, u32[]{:S(2)}, u32[]{:S(2)}) async-start(f32[8,32,256]{2,1,0:T(8,128)} %copy.120), calls=%async_computation.2 | async-start | bytes 524288 | tf_op jit(solution)/shard_map/all_to_all | solution.py:136
  140.4 75.8 %reduce-scatter.2.cloned.1.call-start = ((), (), s32[]{:S(2)}) async-start(), calls=%async_computation.5 | async-start | bytes 1769472 | tf_op jit(solution)/shard_map/reduce_scatter | solution.py:152
  (15 other events, 26.6 us)
Sparse Core Ops, SparseCore 0:
  30.7 20.9 all-gather.1
  152.3 63.7 reduce-scatter.1
where the time goes:
time: 227 us; the launch traced here: 225 us
  waiting for transfers between devices  73.1 us (32%)
  matrix products  62.1 us (27%)
  local copies, waits for them, and re-layouts  44.4 us (20%)
  starting transfers between devices  16.9 us (7%)
  between operations  14.2 us (6%)
  other arithmetic  10.4 us (5%)
  loops' own time  3.57 us (2%)
    reduce_scatter x1, waiting for transfers between devices, per_device(): lax.psum_scatter(lax.dot_general(full_input, key_grad, (((0,), (0,)), (()...  58.9 us
    unnamed x22, local copies, waits for them, and re-layouts  11.4 us
    reshape x4, local copies, waits for them, and re-layouts, one_block(): key_sel_grad.reshape(NSEL, KB, half_width)  8.17 us
    all_to_all x1, waiting for transfers between devices, per_device(): lax.all_to_all(per_owner.reshape(axis_count, KB, pair_width), 'kv', split...  7.9 us
    dot_general x4, matrix products, one_block(): jnp.einsum('qhgk,khd->qhgd', slope_own, key_own, preferred_element_type=j...  7.34 us
    all_to_all x1, starting transfers between devices, per_device(): lax.all_to_all(wanted[:, None], 'kv', split_axis=0, concat_axis=0, tiled=...  7.31 us
    dynamic_update_slice x8, other arithmetic, per_device(): lax.map(one_block, (query_parts, grad_parts, sum_parts, slot_owner, usabl...  6.22 us
    all_to_all x1, starting transfers between devices, per_device(): lax.all_to_all(per_owner.reshape(axis_count, KB, pair_width), 'kv', split...  5.91 us
  transfers between devices with their start and end apart: 5, of which 3 were waited for; matrix products, arithmetic and copies ran while one was open for 47% of the time, Pallas kernels for 0%

commit v1 on v0

--- a/solution.py
+++ b/solution.py
@@ -1,3 +1,4 @@
+import functools
 import jax
 import jax.numpy as jnp
 from jax import lax
@@ -7,6 +8,37 @@
 KB = 32
 QB = 64
 NSEL = 16
+
+
+def _carry_rings(a0, dim_at, frame):
+    r_now, part_now = (a0.shape[:dim_at], a0.shape[dim_at + 1 :])
+    return jnp.moveaxis(a0.reshape(*r_now, frame, -1, *part_now), dim_at, 0)
+
+
+def _order_pages(incoming_x, pos_dim):
+    incoming_x = jnp.moveaxis(incoming_x, 0, pos_dim)
+    state_next = incoming_x.shape
+    return incoming_x.reshape(
+        *state_next[:pos_dim],
+        state_next[pos_dim] * state_next[pos_dim + 1],
+        *state_next[pos_dim + 2 :]
+    )
+
+
+def table_expand(my_data, group_axis, local_block, work_x):
+    prior, new = (lax.axis_size(group_axis), lax.axis_index(group_axis))
+    parts_out = _carry_rings(my_data, local_block, prior)
+    windows = [parts_out[new]]
+    for c in range(1, prior):
+        e_next = parts_out[new ^ c]
+        windows.append(
+            lax.ppermute(e_next, group_axis, [(tick, tick ^ c) for tick in range(prior)])
+        )
+    parts_out = jnp.stack(windows, axis=0)[new ^ jnp.arange(prior)]
+    return _order_pages(parts_out, work_x)
+
+
+extend_the_figure = functools.partial(table_expand, group_axis="kv", local_block=0, work_x=0)
 
 
 def per_device(queries, key_vectors, value_vectors, log_sums, out_grad, layer_input, chosen):
@@ -27,7 +59,7 @@
     within = chosen - chosen // blocks_here * blocks_here
     matched = owner_of[:, :, None] == owners[None, None, :]
     wanted = jnp.max(jnp.where(matched, within[:, :, None], -1), axis=(0, 1))
-    incoming = lax.all_to_all(wanted[:, None], "kv", split_axis=0, concat_axis=0, tiled=True)[:, 0]
+    incoming = extend_the_figure(wanted[:, None])[:, 0]
     blocks = paired.reshape(blocks_here, KB, pair_width)
     outgoing = jnp.where(
         (incoming >= 0)[:, None, None],

time: 227 us -> 236 us (1.040)
  local copies, waits for them, and re-layouts: 44.4 us -> 49.7 us
  starting transfers between devices: 16.9 us -> 22.2 us
    ppermute x0 -> x7, starting transfers between devices: none -> 12.4 us  [table_expand(): lax.ppermute(e_next, group_axis, [(tick, tick ^ c) for tick in range(prio...]
    all_to_all x1 -> x0, starting transfers between devices: 7.31 us -> none  [per_device(): lax.all_to_all(wanted[:, None], 'kv', split_axis=0, concat_axis=0, tiled=...]
    all_to_all x1 -> x0, waiting for transfers between devices: 5.53 us -> none  [per_device(): lax.all_to_all(wanted[:, None], 'kv', split_axis=0, concat_axis=0, tiled=...]
    another operation x0 -> x1, local copies, waits for them, and re-layouts: none -> 5.27 us  [table_expand(): parts_out = jnp.stack(windows, axis=0)[new ^ jnp.arange(prior)]]
    ppermute x0 -> x7, waiting for transfers between devices: none -> 4.53 us  [table_expand(): lax.ppermute(e_next, group_axis, [(tick, tick ^ c) for tick in range(prio...]
    unnamed x22 -> x24, local copies, waits for them, and re-layouts: 11.4 us -> 10.5 us
  transfers between devices with their start and end apart: 5 -> 11, of which waited for: 3 -> 5; matrix products, arithmetic and copies ran while one was open for 47% -> 45% of each run, Pallas kernels for 0% -> 0%
where the time goes in v1:
time: 236 us; the launch traced here: 234 us
  waiting for transfers between devices  72 us (31%)
  matrix products  62.1 us (26%)
  local copies, waits for them, and re-layouts  49.7 us (21%)
  starting transfers between devices  22.2 us (9%)
  between operations  14.3 us (6%)
  other arithmetic  9.91 us (4%)
  loops' own time  3.57 us (2%)
    reduce_scatter x1, waiting for transfers between devices, per_device(): lax.psum_scatter(lax.dot_general(full_input, key_grad, (((0,), (0,)), (()...  58.9 us
    ppermute x7, starting transfers between devices, table_expand(): lax.ppermute(e_next, group_axis, [(tick, tick ^ c) for tick in range(prio...  12.4 us
    unnamed x24, local copies, waits for them, and re-layouts  10.5 us
    reshape x4, local copies, waits for them, and re-layouts, one_block(): key_sel_grad.reshape(NSEL, KB, half_width)  8.19 us
    all_to_all x1, waiting for transfers between devices, per_device(): lax.all_to_all(per_owner.reshape(axis_count, KB, pair_width), 'kv', split...  7.9 us
    dot_general x4, matrix products, one_block(): jnp.einsum('qhgk,khd->qhgd', slope_own, key_own, preferred_element_type=j...  7.41 us
    dynamic_update_slice x8, other arithmetic, per_device(): lax.map(one_block, (query_parts, grad_parts, sum_parts, slot_owner, usabl...  6.28 us
    all_to_all x1, starting transfers between devices, per_device(): lax.all_to_all(per_owner.reshape(axis_count, KB, pair_width), 'kv', split...  5.96 us
  transfers between devices with their start and end apart: 11, of which 5 were waited for; matrix products, arithmetic and copies ran while one was open for 45% of the time, Pallas kernels for 0%

profile of v1, /device:TPU:0, one launch (start us, length us, event | category | flops | bytes accessed | tf_op | source)
XLA Modules:
  0.0 233.8 jit_solution(14263770835586245475)
XLA Ops:
  9.4 5.0 %collective-permute-start.4 = (s32[1,1]{1,0:T(1,128)}, s32[1,1]{1,0:T(1,128)}, u32[]{:S(2)}, u32[]{:S(2)}) collective-permute-start(s32[1,1]{1,0:T(1,128)} %bitcast.9), channel_id=1, source_target_pairs={{0,20},{4,16},{8,28},{12,24},{16,4},{20,0},{24,12},{28,8},{1,21},{... | collective-permute-start | bytes 20 | tf_op jit(solution)/shard_map/ppermute | solution.py:35
  15.7 2.4 %collective-permute-start.6 = (s32[1,1]{1,0:T(1,128)}, s32[1,1]{1,0:T(1,128)}, u32[]{:S(2)}, u32[]{:S(2)}) collective-permute-start(s32[1,1]{1,0:T(1,128)} %bitcast.13), channel_id=1, source_target_pairs={{0,28},{4,24},{8,20},{12,16},{16,12},{20,8},{24,4},{28,0},{1,29},{... | collective-permute-start | bytes 20 | tf_op jit(solution)/shard_map/ppermute | solution.py:35
  18.1 1.5 collective-permute-start
  20.6 2.0 collective-permute-start.2
  23.4 1.7 collective-permute-done.2
  25.1 2.0 collective-permute-done.3
  27.2 5.3 %stack.31 = s32[8,1,1]{0,2,1:T(1,128)S(1)} concatenate(s32[1,1,1]{0,2,1:T(1,128)} %bitcast, s32[1,1,1]{0,2,1:T(1,128)} %bitcast.2, s32[1,1,1]{0,2,1:T(1,128)} %bitcast.4, s32[1,1,1]{0,2,1:T(1,128)} %bitcast.6, s32[1,1,1]{0,2,1:T(1,128)} %bitcast.8, s32[1,1,1]{0,2,1:T(1,128)} %bitcast.10, s32[1,1,1]{0,2,1:T(1,128)} %bitcast.12, s32[1,1,1]{0,2,1:T(1,128)} %bitcast.14), dimensions={0} | concatenate | bytes 64 | tf_op jit(solution)/shard_map/stack | solution.py:37
  34.4 3.6 %all-to-all-start = ((bf16[8,32,256]{2,1,0:T(8,128)(2,1)}), bf16[8,32,256]{2,1,0:T(8,128)(2,1)S(1)}, u32[]{:S(2)}, u32[]{:S(2)}) async-start(bf16[8,32,256]{2,1,0:T(8,128)(2,1)} %broadcast_select_fusion), calls=%async_computation | async-start | bytes 262144 | tf_op jit(solution)/shard_map/all_to_all | solution.py:69
  45.9 93.4 %while.18 = (s32[]{:T(128)}, bf16[4,64,2,6,64]{1,4,3,2,0:T(8,128)(2,1)}, f32[4,16,32,256]{3,2,1,0:T(8,128)}, f32[4,256,256]{1,2,0:T(8,128)}, s32[4,16]{1,0:T(4,1...) while((s32[]{:T(128)}, ...), condition=%wide.region_3.4_spmd.clone.clone, body=%wide.region_1.3_spmd.clone.clone.sunk | while | flops 458359424 | bytes 25241412 | solution.py:155
  57.5 2.1 reshape.270
  67.4 1.8 fusion.159
  80.8 2.0 reshape.270
  90.7 1.9 fusion.159
  104.2 2.0 reshape.270
  114.0 1.9 fusion.159
  127.5 2.0 reshape.270
  137.4 1.8 fusion.159
  139.3 3.5 %fusion.66 = f32[8,32,256]{2,0,1:T(8,128)S(1)} fusion(s32[64]{0:T(128)} %eq.48, pred[64]{0:T(512)(128)(4,1)} %and.19, f32[8,8,32,256]{3,2,1,0:T(8,128)} %bitcast.292), kind=kOutput, calls=%fused_computation.91 | convolution fusion | flops 50332672 | bytes 2359616 | tf_op jit(solution)/shard_map/so,sr->or/dot_general | solution.py:162
  143.6 6.0 %all-to-all-start.1 = ((f32[8,32,256]{2,1,0:T(8,128)}), f32[8,32,256]{2,1,0:T(8,128)S(1)}, u32[]{:S(2)}, u32[]{:S(2)}) async-start(f32[8,32,256]{2,1,0:T(8,128)} %copy.91), calls=%async_computation.1 | async-start | bytes 524288 | tf_op jit(solution)/shard_map/all_to_all | solution.py:168
  149.9 7.9 %all-to-all-done.1 = f32[8,32,256]{2,1,0:T(8,128)S(1)} async-done(((f32[8,32,256]{2,1,0:T(8,128)}), f32[8,32,256]{2,1,0:T(8,128)S(1)}, u32[]{:S(2)}, u32[]{:S(2)}) %all-to-all-start.1) | async-done | bytes 262176 | tf_op jit(solution)/shard_map/all_to_all | solution.py:168
  158.4 2.9 %convolution_bitcast_fusion.8 = f32[3072,128]{0,1:T(8,128)} fusion(bf16[256,3072]{1,0:T(8,128)(2,1)} %all-gather.2.cloned.1.call-done, bf16[256,256]{0,1:T(8,128)(2,1)S(1)} %add_convert_fusion), kind=kOutput, calls=%fused_computation.90 | convolution fusion | flops 201326592 | bytes 3211264 | tf_op jit(solution)/shard_map/dot_general | solution.py:185
  163.5 1.4 reshape.260
  166.3 58.9 %reduce-scatter.2.cloned.1.call-done = f32[384,128]{0,1:T(8,128)} async-done(((f32[3072,128]{0,1:T(8,128)}), f32[384,128]{0,1:T(8,128)}) %reduce-scatter.2.cloned.1.call-update) | async-done | bytes 196624 | tf_op jit(solution)/shard_map/reduce_scatter | solution.py:184
  225.2 1.7 copy.96
  (248 shorter events, 94.4 us)
Async XLA Ops:
  7.2 31.6 %copy-start.7 = (bf16[256,128]{1,0:T(8,128)(2,1)S(1)}, bf16[256,128]{1,0:T(8,128)(2,1)}, u32[]{:S(2)}) copy-start(bf16[256,128]{1,0:T(8,128)(2,1)} %param.10) | copy-start | bytes 196612
  7.2 32.3 %copy-start.8 = (bf16[256,128]{1,0:T(8,128)(2,1)S(1)}, bf16[256,128]{1,0:T(8,128)(2,1)}, u32[]{:S(2)}) copy-start(bf16[256,128]{1,0:T(8,128)(2,1)} %param.11) | copy-start | bytes 196612
  7.2 33.1 %copy-start.5 = (bf16[256,768]{1,0:T(8,128)(2,1)S(1)}, bf16[256,768]{1,0:T(8,128)(2,1)}, u32[]{:S(2)}) copy-start(bf16[256,768]{1,0:T(8,128)(2,1)} %param.9) | copy-start | bytes 1179652
  9.4 11.2 %collective-permute-start.4 = (s32[1,1]{1,0:T(1,128)}, s32[1,1]{1,0:T(1,128)}, u32[]{:S(2)}, u32[]{:S(2)}) collective-permute-start(s32[1,1]{1,0:T(1,128)} %bitcast.9), channel_id=1, source_target_pairs={{0,20},{4,16},{8,28},{12,24},{16,4},{20,0},{24,12},{28,8},{1,21},{... | collective-permute-start | bytes 20 | tf_op jit(solution)/shard_map/ppermute | solution.py:35
  14.4 8.2 %collective-permute-start.5 = (s32[1,1]{1,0:T(1,128)}, s32[1,1]{1,0:T(1,128)}, u32[]{:S(2)}, u32[]{:S(2)}) collective-permute-start(s32[1,1]{1,0:T(1,128)} %bitcast.11), channel_id=1, source_target_pairs={{0,24},{4,28},{8,16},{12,20},{16,8},{20,12},{24,0},{28,4},{1,25},{... | collective-permute-start | bytes 20 | tf_op jit(solution)/shard_map/ppermute | solution.py:35
  15.7 6.9 %collective-permute-start.6 = (s32[1,1]{1,0:T(1,128)}, s32[1,1]{1,0:T(1,128)}, u32[]{:S(2)}, u32[]{:S(2)}) collective-permute-start(s32[1,1]{1,0:T(1,128)} %bitcast.13), channel_id=1, source_target_pairs={{0,28},{4,24},{8,20},{12,16},{16,12},{20,8},{24,4},{28,0},{1,29},{... | collective-permute-start | bytes 20 | tf_op jit(solution)/shard_map/ppermute | solution.py:35
  18.1 4.5 %collective-permute-start = (s32[1,1]{1,0:T(1,128)}, s32[1,1]{1,0:T(1,128)}, u32[]{:S(2)}, u32[]{:S(2)}) collective-permute-start(s32[1,1]{1,0:T(1,128)} %bitcast.1), channel_id=1, source_target_pairs={{0,4},{4,0},{8,12},{12,8},{16,20},{20,16},{24,28},{28,24},{1,5},{5... | collective-permute-start | bytes 20 | tf_op jit(solution)/shard_map/ppermute | solution.py:35
  19.7 3.7 %collective-permute-start.1 = (s32[1,1]{1,0:T(1,128)}, s32[1,1]{1,0:T(1,128)}, u32[]{:S(2)}, u32[]{:S(2)}) collective-permute-start(s32[1,1]{1,0:T(1,128)} %bitcast.3), channel_id=1, source_target_pairs={{0,8},{4,12},{8,0},{12,4},{16,24},{20,28},{24,16},{28,20},{1,9},{5... | collective-permute-start | bytes 20 | tf_op jit(solution)/shard_map/ppermute | solution.py:35
  20.6 4.5 %collective-permute-start.2 = (s32[1,1]{1,0:T(1,128)}, s32[1,1]{1,0:T(1,128)}, u32[]{:S(2)}, u32[]{:S(2)}) collective-permute-start(s32[1,1]{1,0:T(1,128)} %bitcast.5), channel_id=1, source_target_pairs={{0,12},{4,8},{8,4},{12,0},{16,28},{20,24},{24,20},{28,16},{1,13},{... | collective-permute-start | bytes 20 | tf_op jit(solution)/shard_map/ppermute | solution.py:35
  22.6 4.6 %collective-permute-start.3 = (s32[1,1]{1,0:T(1,128)}, s32[1,1]{1,0:T(1,128)}, u32[]{:S(2)}, u32[]{:S(2)}) collective-permute-start(s32[1,1]{1,0:T(1,128)} %bitcast.7), channel_id=1, source_target_pairs={{0,16},{4,20},{8,24},{12,28},{16,0},{20,4},{24,8},{28,12},{1,17},{... | collective-permute-start | bytes 20 | tf_op jit(solution)/shard_map/ppermute | solution.py:35
  34.4 11.5 %all-to-all-start = ((bf16[8,32,256]{2,1,0:T(8,128)(2,1)}), bf16[8,32,256]{2,1,0:T(8,128)(2,1)S(1)}, u32[]{:S(2)}, u32[]{:S(2)}) async-start(bf16[8,32,256]{2,1,0:T(8,128)(2,1)} %broadcast_select_fusion), calls=%async_computation | async-start | bytes 262144 | tf_op jit(solution)/shard_map/all_to_all | solution.py:69
  38.0 120.4 %all-gather.2.cloned.1.call-start = ((), (), s32[]{:S(2)}) async-start(), calls=%async_computation.3 | async-start | bytes 1966080 | tf_op jit(solution)/shard_map/all_gather | solution.py:183
  45.9 4.2 %copy-start.12 = (s32[4]{0:T(128)}, s32[4]{0:T(128)S(1)}, u32[]{:S(2)}) copy-start(s32[4]{0:T(128)S(1)} %get-tuple-element.478) | copy-start | bytes 52 | tf_op jit(solution)/shard_map/while
  62.6 4.3 %copy-start.2 = (bf16[512,1,2,64]{0,3,2,1:T(8,128)(2,1)S(1)}, bf16[512,1,2,64]{0,3,2,1:T(8,128)(2,1)}, u32[]{:S(2)}) copy-start(bf16[512,1,2,64]{0,3,2,1:T(8,128)(2,1)} %copy-done.1) | copy-start | bytes 393220 | tf_op jit(solution)/shard_map/while
  69.2 4.2 %copy-start.12 = (s32[4]{0:T(128)}, s32[4]{0:T(128)S(1)}, u32[]{:S(2)}) copy-start(s32[4]{0:T(128)S(1)} %get-tuple-element.478) | copy-start | bytes 52 | tf_op jit(solution)/shard_map/while
  85.9 4.3 %copy-start.2 = (bf16[512,1,2,64]{0,3,2,1:T(8,128)(2,1)S(1)}, bf16[512,1,2,64]{0,3,2,1:T(8,128)(2,1)}, u32[]{:S(2)}) copy-start(bf16[512,1,2,64]{0,3,2,1:T(8,128)(2,1)} %copy-done.1) | copy-start | bytes 393220 | tf_op jit(solution)/shard_map/while
  92.6 4.2 %copy-start.12 = (s32[4]{0:T(128)}, s32[4]{0:T(128)S(1)}, u32[]{:S(2)}) copy-start(s32[4]{0:T(128)S(1)} %get-tuple-element.478) | copy-start | bytes 52 | tf_op jit(solution)/shard_map/while
  109.2 4.3 %copy-start.2 = (bf16[512,1,2,64]{0,3,2,1:T(8,128)(2,1)S(1)}, bf16[512,1,2,64]{0,3,2,1:T(8,128)(2,1)}, u32[]{:S(2)}) copy-start(bf16[512,1,2,64]{0,3,2,1:T(8,128)(2,1)} %copy-done.1) | copy-start | bytes 393220 | tf_op jit(solution)/shard_map/while
  112.8 3.1 %copy-start.10 = (f32[4,64,2,6]{1,0,3,2:T(4,128)S(1)}, f32[4,64,2,6]{1,0,3,2:T(4,128)}, u32[]{:S(2)}) copy-start(f32[4,64,2,6]{1,0,3,2:T(4,128)} %copy-done.9) | copy-start | bytes 36868 | tf_op jit(solution)/shard_map/while
  115.9 4.2 %copy-start.12 = (s32[4]{0:T(128)}, s32[4]{0:T(128)S(1)}, u32[]{:S(2)}) copy-start(s32[4]{0:T(128)S(1)} %get-tuple-element.478) | copy-start | bytes 52 | tf_op jit(solution)/shard_map/while
  132.6 4.3 %copy-start.2 = (bf16[512,1,2,64]{0,3,2,1:T(8,128)(2,1)S(1)}, bf16[512,1,2,64]{0,3,2,1:T(8,128)(2,1)}, u32[]{:S(2)}) copy-start(bf16[512,1,2,64]{0,3,2,1:T(8,128)(2,1)} %copy-done.1) | copy-start | bytes 393220 | tf_op jit(solution)/shard_map/while
  139.2 10.5 %copy-start.3 = (f32[4,256,256]{1,2,0:T(8,128)S(1)}, f32[4,256,256]{1,2,0:T(8,128)}, u32[]{:S(2)}) copy-start(f32[4,256,256]{1,2,0:T(8,128)} %get-tuple-element.178) | copy-start | bytes 3145732
  143.6 14.2 %all-to-all-start.1 = ((f32[8,32,256]{2,1,0:T(8,128)}), f32[8,32,256]{2,1,0:T(8,128)S(1)}, u32[]{:S(2)}, u32[]{:S(2)}) async-start(f32[8,32,256]{2,1,0:T(8,128)} %copy.91), calls=%async_computation.1 | async-start | bytes 524288 | tf_op jit(solution)/shard_map/all_to_all | solution.py:168
  149.5 75.7 %reduce-scatter.2.cloned.1.call-start = ((), (), s32[]{:S(2)}) async-start(), calls=%async_computation.4 | async-start | bytes 1769472 | tf_op jit(solution)/shard_map/reduce_scatter | solution.py:184
  (22 other events, 48.5 us)
Sparse Core Ops, SparseCore 0:
  40.4 21.0 all-gather.1
  161.5 63.6 reduce-scatter.1
